TPU v7x, 32 devices: a whole 2x2x4 slice. The times are simulated.
32 devices in a mesh: sp: 8 (over z, y), tp: 4 (over x, core).
Axes of the slice: x: 2, y: 2, z: 4, core: 2. Of those that a mesh axis runs over, the one named last changes fastest.
Arguments:
- tokens: bfloat16 [6144, 4096], P('sp', 'tp'), may hold values from -6 to 6
- in_proj: bfloat16 [3, 4096, 1024], P(None, 'tp', 'sp'), may hold values from -0.09375 to 0.09375
- group_mix: bfloat16 [3, 4, 256, 256], replicated, may hold values from -0.375 to 0.375
- pool_gain: float32 [3, 1024], replicated, may hold values from 0.1 to 1.9
- out_proj: bfloat16 [3, 1024, 4096], P(None, 'sp', 'tp'), may hold values from -0.1875 to 0.1875
- norm_gain: float32 [3, 4096], P(None, 'tp'), may hold values from 0.25 to 3
- norm_bias: float32 [3, 4096], P(None, 'tp'), may hold values from -1.5 to 1.5
Outputs:
- stream_out: bfloat16 [6144, 4096], P('sp', 'tp')
All inputs are finite; a program needn't handle non-finite values.
Results may differ from a plain program's by a relative error of at most 0.017.
Values may be sent and summed in bfloat16 or wider, within the bound.
A program may use at most 128 MiB of HBM per device.

v0:
```python
import jax
import jax.numpy as jnp
from jax import lax
from jax.sharding import PartitionSpec as P

pool_windows = (2, 4, 8, 16)
norm_eps = 1e-05


def padded(array, sides, width):
    for axis, dim in sides:
        devices, length = (lax.axis_size(axis), array.shape[dim])
        up = [(i, (i + 1) % devices) for i in range(devices - 1)]
        down = [(j, i) for i, j in up]
        last = lax.slice_in_dim(array, length - width, length, axis=dim)
        leading = lax.slice_in_dim(array, 0, width, axis=dim)
        before = lax.ppermute(last, axis, up)
        after = lax.ppermute(leading, axis, down)
        array = jnp.concatenate([before, array, after], axis=dim)
    return array


def on_device(tokens, in_proj, group_mix, pool_gain, out_proj, norm_gain, norm_bias):
    rows_dev = tokens.shape[0]
    feat_dev = tokens.shape[1]
    layer_count = in_proj.shape[0]
    pool_width = in_proj.shape[2] * lax.axis_size("sp")
    chan_share = pool_width // lax.axis_size("tp")
    group_width = group_mix.shape[2]
    model_width = feat_dev * lax.axis_size("tp")
    residual_scale = (2.0 * layer_count) ** 0.25
    fringe_width = max(pool_windows) // 2
    seq_length = rows_dev * lax.axis_size("sp")
    positions = lax.axis_index("sp") * rows_dev + jnp.arange(rows_dev)
    chan_groups = (lax.axis_index("tp") * chan_share + jnp.arange(chan_share)) // group_width
    in_all, out_all = (
        lax.all_gather(in_proj, "sp", axis=2, tiled=True),
        lax.all_gather(out_proj, "sp", axis=1, tiled=True),
    )
    stream = tokens
    for layer_idx in range(layer_count):
        in_block = in_all[layer_idx]
        out_block = out_all[layer_idx]
        projected = lax.psum_scatter(
            lax.dot_general(
                in_block, stream, (((0,), (1,)), ((), ())), preferred_element_type=jnp.float32
            ).astype(jnp.bfloat16),
            "tp",
            scatter_dimension=0,
            tiled=True,
        )
        extended = padded(projected, (("sp", 1),), fringe_width)
        ext_float = extended.astype(jnp.float32)
        pooled = jnp.zeros((chan_share, rows_dev), jnp.float32)
        for group_idx in range(4):
            own_rows = (chan_groups == group_idx)[:, None]
            span_len = pool_windows[group_idx]
            before = span_len // 2
            after = span_len - before
            window_total = jnp.zeros((ext_float.shape[0], rows_dev), jnp.float32)
            for offset in range(-before, after):
                window_total = (
                    window_total
                    + ext_float[:, fringe_width + offset : fringe_width + offset + rows_dev]
                )
            low_edge = jnp.clip(positions - before, 0, seq_length)
            high_edge = jnp.clip(positions + after, 0, seq_length)
            pooled = jnp.where(
                own_rows, window_total / (high_edge - low_edge).astype(jnp.float32)[None, :], pooled
            )
        differ = (pooled - projected.astype(jnp.float32)).astype(jnp.bfloat16)
        all_differ = lax.all_gather(differ, "tp", axis=0, tiled=True)
        grouped = all_differ.reshape(4, group_width, rows_dev)
        mixed_all = jnp.einsum(
            "gcd,gct->gdt", group_mix[layer_idx], grouped, preferred_element_type=jnp.float32
        ).reshape(pool_width, rows_dev)
        mixed_all = (mixed_all * pool_gain[layer_idx][:, None]).astype(jnp.bfloat16)
        branch = lax.dot_general(
            mixed_all, out_block, (((0,), (0,)), ((), ())), preferred_element_type=jnp.float32
        )
        resid = residual_scale * stream.astype(jnp.float32) + branch
        row_sums, squares = lax.psum((jnp.sum(resid, axis=1), jnp.sum(resid * resid, axis=1)), "tp")
        row_mean = row_sums / model_width
        row_var = squares / model_width - row_mean * row_mean
        normed = (resid - row_mean[:, None]) * lax.rsqrt(row_var[:, None] + norm_eps)
        stream = (normed * norm_gain[layer_idx][None, :] + norm_bias[layer_idx][None, :]).astype(
            jnp.bfloat16
        )
    return stream


def solution(mesh):
    in_specs = (
        P("sp", "tp"),
        P(None, "tp", "sp"),
        P(),
        P(),
        P(None, "sp", "tp"),
        P(None, "tp"),
        P(None, "tp"),
    )
    out_specs = P("sp", "tp")
    return jax.shard_map(
        on_device, mesh=mesh, in_specs=in_specs, out_specs=out_specs, check_vma=False
    )
```

profile of v0, /device:TPU:0, one launch (start us, length us, event | category | flops | bytes accessed | tf_op | source)
XLA Modules:
  0.0 468.3 jit_solution(7111326799867742258)
XLA Ops:
  6.5 0.7 all-gather.6.cloned.1.call-update
  7.3 0.0 reduce-scatter.4.cloned.1.call-start
  7.3 104.3 %all-gather.6.cloned.1.call-done = bf16[3,1024,1024]{2,1,0:T(8,128)(2,1)} async-done(((bf16[3,1024,128]{2,1,0:T(8,128)(2,1)}), bf16[3,1024,1024]{2,1,0:T(8,128)(2,1)}) %all-gather.6.cloned.1.call-update) | async-done | bytes 6291472 | tf_op jit(solution)/shard_map/all_gather | solution.py:37
  111.6 5.0 %fusion.6 = bf16[1024,768]{1,0:T(8,128)(2,1)} fusion(bf16[768,1024]{1,0:T(8,128)(2,1)} %param.7, bf16[3,1024,1024]{2,1,0:T(8,128)(2,1)} %all-gather.6.cloned.1.call-done), kind=kOutput, calls=%fused_computation.24 | convolution fusion | flops 1611399168 | bytes 5242880 | tf_op jit(solution)/shard_map/dot_general | solution.py:45
  116.6 0.0 reduce-scatter.4.cloned.1.call-update
  116.7 0.0 all-gather.8.cloned.1.call-start
  116.8 26.3 %reduce-scatter.4.cloned.1.call-done = bf16[256,768]{1,0:T(8,128)(2,1)} async-done(((bf16[1024,768]{1,0:T(8,128)(2,1)}), bf16[256,768]{1,0:T(8,128)(2,1)}) %reduce-scatter.4.cloned.1.call-update) | async-done | bytes 393232 | tf_op jit(solution)/shard_map/reduce_scatter | solution.py:44
  143.0 1.0 fusion.58
  144.0 3.4 collective-permute-start
  147.4 1.3 collective-permute-start.1
  148.7 0.6 collective-permute-done
  149.3 4.3 collective-permute-done.1
  153.6 1.2 maximum_convert_fusion
  154.8 0.0 copy-start.1
  154.8 0.0 copy-start.2
  154.8 0.0 copy-start.3
  154.8 0.0 copy-start
  154.8 5.1 %fusion.44 = bf16[256,768]{1,0:T(8,128)(2,1)} fusion(bf16[256,768]{1,0:T(8,128)(2,1)} %reduce-scatter.4.cloned.1.call-done, f32[256,784]{1,0:T(8,128)S(1)} %maximum_convert_fusion, f32[768]{0:T(1024)S(1)} %get-tuple-element.41, f32[768]{0:T(1024)S(1)} %get-tuple-element.42, f32[768]{0:T(1024)S(1)} %get-tuple-element.43, f32[768]{0:T(1024)S(1)} %get-tuple-element.44, ...), kind=kLoop, calls=%fused_computation.83 | loop fusion | flops 7274496 | bytes 13382656 | tf_op jit(solution)/shard_map/convert_element_type | solution.py:71
  159.9 0.0 all-gather.8.cloned.1.call-update
  159.9 0.0 all-gather.10.cloned.1.call-start
  160.0 0.5 all-gather.10.cloned.1.call-update
  160.5 0.0 reduce-scatter.6.cloned.1.call-start
  160.6 0.0 copy-done.2
  160.7 19.0 %all-gather.8.cloned.1.call-done = bf16[1024,768]{1,0:T(8,128)(2,1)} async-done(((bf16[256,768]{1,0:T(8,128)(2,1)}), bf16[1024,768]{1,0:T(8,128)(2,1)}) %all-gather.8.cloned.1.call-update) | async-done | bytes 1572880 | tf_op jit(solution)/shard_map/all_gather | solution.py:72
  179.7 2.0 multiply_convert_fusion.2
  181.7 98.7 %all-gather.10.cloned.1.call-done = bf16[3,1024,1024]{2,1,0:T(8,128)(2,1)} async-done(((bf16[3,128,1024]{2,1,0:T(8,128)(2,1)}), bf16[3,1024,1024]{2,1,0:T(8,128)(2,1)}) %all-gather.10.cloned.1.call-update) | async-done | bytes 6291472 | tf_op jit(solution)/shard_map/all_gather | solution.py:38
  280.5 5.8 %fusion.55 = (f32[768]{0:T(1024)S(1)}, f32[768]{0:T(1024)S(1)}, f32[768,1024]{1,0:T(8,128)}) fusion(bf16[1024,768]{1,0:T(8,128)(2,1)S(1)} %bitcast.86, bf16[3,1024,1024]{2,1,0:T(8,128)(2,1)} %all-gather.10.cloned.1.call-done, bf16[768,1024]{1,0:T(8,128)(2,1)} %param.7), kind=kOutput, calls=%fused_computation.119 | convolution fusion | flops 1615329792 | bytes 8394752 | tf_op jit(solution)/shard_map/dot_general | solution.py:78
  286.2 5.7 %all-reduce.2 = (f32[768]{0:T(1024)S(1)}, f32[768]{0:T(1024)S(1)}) all-reduce(f32[768]{0:T(1024)S(1)} %get-tuple-element.10, f32[768]{0:T(1024)S(1)} %get-tuple-element.9), channel_id=1, replica_groups=mesh['sp'=8,'tp'=4] {'tp'}, use_global_device_ids=true, to_apply=%region_4.5 | all-reduce | flops 1536 | bytes 12288 | tf_op jit(solution)/shard_map/psum | solution.py:82
  292.0 5.9 %fusion.10 = bf16[1024,768]{1,0:T(8,128)(2,1)} fusion(bf16[3,1024,1024]{2,1,0:T(8,128)(2,1)} %all-gather.6.cloned.1.call-done, f32[768,1024]{1,0:T(8,128)} %get-tuple-element.38, f32[1024]{0:T(1024)S(1)} %bitcast.95, f32[1024]{0:T(1024)S(1)} %bitcast.93, f32[768]{0:T(1024)S(1)} %get-tuple-element.37, f32[768]{0:T(1024)S(1)} %get-tuple-element.36), kind=kOutput, calls=%fused_computation.28 | convolution fusion | flops 1615331328 | bytes 6830080 | tf_op jit(solution)/shard_map/dot_general | solution.py:45
  297.9 0.0 reduce-scatter.6.cloned.1.call-update
  297.9 0.0 all-gather.12.cloned.1.call-start
  298.0 26.6 %reduce-scatter.6.cloned.1.call-done = bf16[256,768]{1,0:T(8,128)(2,1)} async-done(((bf16[1024,768]{1,0:T(8,128)(2,1)}), bf16[256,768]{1,0:T(8,128)(2,1)}) %reduce-scatter.6.cloned.1.call-update) | async-done | bytes 393232 | tf_op jit(solution)/shard_map/reduce_scatter | solution.py:44
  324.6 1.0 fusion.57
  325.6 3.4 collective-permute-start.2
  328.9 1.3 collective-permute-start.3
  330.2 0.6 collective-permute-done.2
  330.8 4.3 collective-permute-done.3
  335.1 1.2 maximum_convert_fusion.1
  336.3 5.0 %fusion.45 = bf16[256,768]{1,0:T(8,128)(2,1)} fusion(bf16[256,768]{1,0:T(8,128)(2,1)} %reduce-scatter.6.cloned.1.call-done, f32[256,784]{1,0:T(8,128)S(1)} %maximum_convert_fusion.1, f32[768]{0:T(1024)S(1)} %get-tuple-element.41, f32[768]{0:T(1024)S(1)} %get-tuple-element.42, f32[768]{0:T(1024)S(1)} %get-tuple-element.43, f32[768]{0:T(1024)S(1)} %get-tuple-element.44, ...), kind=kLoop, calls=%fused_computation.84 | loop fusion | flops 7274496 | bytes 13382656 | tf_op jit(solution)/shard_map/convert_element_type | solution.py:71
  341.3 0.0 all-gather.12.cloned.1.call-update
  341.3 0.2 reduce-scatter.8.cloned.1.call-start
  341.5 19.5 %all-gather.12.cloned.1.call-done = bf16[1024,768]{1,0:T(8,128)(2,1)} async-done(((bf16[256,768]{1,0:T(8,128)(2,1)}), bf16[1024,768]{1,0:T(8,128)(2,1)}) %all-gather.12.cloned.1.call-update) | async-done | bytes 1572880 | tf_op jit(solution)/shard_map/all_gather | solution.py:72
  361.1 2.2 multiply_convert_fusion.1
  363.3 0.2 copy-done.4
  363.5 5.9 %fusion.54 = (f32[768]{0:T(1024)S(1)}, f32[768]{0:T(1024)S(1)}, f32[768,1024]{1,0:T(8,128)}) fusion(bf16[1024,768]{1,0:T(8,128)(2,1)S(1)} %bitcast.85, bf16[3,1024,1024]{2,1,0:T(8,128)(2,1)} %all-gather.10.cloned.1.call-done, f32[1024]{0:T(1024)S(1)} %bitcast.96, f32[1024]{0:T(1024)S(1)} %bitcast.94, f32[768]{0:T(1024)S(1)} %get-tuple-element.37, ...), kind=kOutput, calls=%fused_computation.118 | convolution fusion | flops 1619261952 | bytes 9981952 | tf_op jit(solution)/shard_map/dot_general | solution.py:78
  369.3 6.0 %all-reduce.1 = (f32[768]{0:T(1024)S(1)}, f32[768]{0:T(1024)S(1)}) all-reduce(f32[768]{0:T(1024)S(1)} %get-tuple-element.8, f32[768]{0:T(1024)S(1)} %get-tuple-element.7), channel_id=1, replica_groups=mesh['sp'=8,'tp'=4] {'tp'}, use_global_device_ids=true, to_apply=%region_9.10 | all-reduce | flops 1536 | bytes 12288 | tf_op jit(solution)/shard_map/psum | solution.py:82
  375.3 5.9 %fusion.9 = bf16[1024,768]{1,0:T(8,128)(2,1)} fusion(bf16[3,1024,1024]{2,1,0:T(8,128)(2,1)} %all-gather.6.cloned.1.call-done, f32[768,1024]{1,0:T(8,128)} %get-tuple-element.39, f32[1024]{0:T(1024)S(1)} %bitcast.91, f32[1024]{0:T(1024)S(1)} %bitcast.89, f32[768]{0:T(1024)S(1)} %get-tuple-element.35, f32[768]{0:T(1024)S(1)} %get-tuple-element.34), kind=kOutput, calls=%fused_computation.27 | convolution fusion | flops 1615331328 | bytes 6830080 | tf_op jit(solution)/shard_map/dot_general | solution.py:45
  381.2 0.0 reduce-scatter.8.cloned.1.call-update
  381.2 0.0 all-gather.14.cloned.1.call-start
  381.3 29.2 %reduce-scatter.8.cloned.1.call-done = bf16[256,768]{1,0:T(8,128)(2,1)} async-done(((bf16[1024,768]{1,0:T(8,128)(2,1)}), bf16[256,768]{1,0:T(8,128)(2,1)}) %reduce-scatter.8.cloned.1.call-update) | async-done | bytes 393232 | tf_op jit(solution)/shard_map/reduce_scatter | solution.py:44
  410.5 1.0 fusion.56
  411.5 3.4 collective-permute-start.4
  414.8 1.3 collective-permute-start.5
  416.1 0.6 collective-permute-done.4
  416.7 4.3 collective-permute-done.5
  421.0 1.2 maximum_convert_fusion.2
  422.2 5.0 %fusion.46 = bf16[256,768]{1,0:T(8,128)(2,1)} fusion(bf16[256,768]{1,0:T(8,128)(2,1)} %reduce-scatter.8.cloned.1.call-done, f32[256,784]{1,0:T(8,128)S(1)} %maximum_convert_fusion.2, f32[768]{0:T(1024)S(1)} %get-tuple-element.41, f32[768]{0:T(1024)S(1)} %get-tuple-element.42, f32[768]{0:T(1024)S(1)} %get-tuple-element.43, f32[768]{0:T(1024)S(1)} %get-tuple-element.44, ...), kind=kLoop, calls=%fused_computation.85 | loop fusion | flops 7274496 | bytes 13382656 | tf_op jit(solution)/shard_map/convert_element_type | solution.py:71
  427.2 0.0 all-gather.14.cloned.1.call-update
  427.2 19.8 %all-gather.14.cloned.1.call-done = bf16[1024,768]{1,0:T(8,128)(2,1)} async-done(((bf16[256,768]{1,0:T(8,128)(2,1)}), bf16[1024,768]{1,0:T(8,128)(2,1)}) %all-gather.14.cloned.1.call-update) | async-done | bytes 1572880 | tf_op jit(solution)/shard_map/all_gather | solution.py:72
  447.0 2.2 multiply_convert_fusion
  449.2 0.2 copy-done.5
  449.4 4.4 fusion.53
  453.7 6.0 %all-reduce = (f32[768]{0:T(1024)S(1)}, f32[768]{0:T(1024)S(1)}) all-reduce(f32[768]{0:T(1024)S(1)} %get-tuple-element.6, f32[768]{0:T(1024)S(1)} %get-tuple-element.5), channel_id=1, replica_groups=mesh['sp'=8,'tp'=4] {'tp'}, use_global_device_ids=true, to_apply=%region_14.15 | all-reduce | flops 1536 | bytes 12288 | tf_op jit(solution)/shard_map/psum | solution.py:82
  459.7 1.7 add_convert_fusion
  (19 shorter events, 0.2 us)
Async XLA Ops:
  6.5 105.1 %all-gather.6.cloned.1.call-start = ((), (), s32[]{:S(2)}) async-start(), calls=%async_computation.3 | async-start | bytes 7077888 | tf_op jit(solution)/shard_map/all_gather | solution.py:37
  7.3 135.8 %reduce-scatter.4.cloned.1.call-start = ((), (), s32[]{:S(2)}) async-start(), calls=%async_computation.4 | async-start | bytes 1966080 | tf_op jit(solution)/shard_map/reduce_scatter | solution.py:44
  116.7 63.0 %all-gather.8.cloned.1.call-start = ((), (), s32[]{:S(2)}) async-start(), calls=%async_computation.5 | async-start | bytes 1966080 | tf_op jit(solution)/shard_map/all_gather | solution.py:72
  144.0 5.3 %collective-permute-start = (bf16[256,8]{1,0:T(8,128)(2,1)S(1)}, bf16[256,8]{1,0:T(8,128)(2,1)S(1)}, u32[]{:S(2)}, u32[]{:S(2)}) collective-permute-start(bf16[256,8]{1,0:T(8,128)(2,1)S(1)} %get-tuple-element.24), channel_id=1, source_target_pairs={{0,4},{4,8},{8,12},{12,16},{16,20},{20,24},{24,28},{1,5},{5,9},{9,... | collective-permute-start | bytes 12296 | tf_op jit(solution)/shard_map/ppermute | solution.py:17
  147.4 6.2 %collective-permute-start.1 = (bf16[256,8]{1,0:T(8,128)(2,1)S(1)}, bf16[256,8]{1,0:T(8,128)(2,1)S(1)}, u32[]{:S(2)}, u32[]{:S(2)}) collective-permute-start(bf16[256,8]{1,0:T(8,128)(2,1)S(1)} %get-tuple-element.25), channel_id=1, source_target_pairs={{4,0},{8,4},{12,8},{16,12},{20,16},{24,20},{28,24},{5,1},{9,5},{13... | collective-permute-start | bytes 12296 | tf_op jit(solution)/shard_map/ppermute | solution.py:18
  154.8 5.8 %copy-start.1 = (f32[3,1024]{1,0:T(4,128)S(1)}, f32[3,1024]{1,0:T(4,128)}, u32[]{:S(2)}) copy-start(f32[3,1024]{1,0:T(4,128)} %param.10) | copy-start | bytes 36868
  154.8 5.8 %copy-start.2 = (f32[3,1024]{1,0:T(4,128)S(1)}, f32[3,1024]{1,0:T(4,128)}, u32[]{:S(2)}) copy-start(f32[3,1024]{1,0:T(4,128)} %param.12) | copy-start | bytes 36868
  154.8 5.8 %copy-start.3 = (f32[3,1024]{1,0:T(4,128)S(1)}, f32[3,1024]{1,0:T(4,128)}, u32[]{:S(2)}) copy-start(f32[3,1024]{1,0:T(4,128)} %param.13) | copy-start | bytes 36868
  154.8 24.9 %copy-start = (bf16[3,4,256,256]{3,2,1,0:T(8,128)(2,1)S(1)}, bf16[3,4,256,256]{3,2,1,0:T(8,128)(2,1)}, u32[]{:S(2)}) copy-start(bf16[3,4,256,256]{3,2,1,0:T(8,128)(2,1)} %param.9) | copy-start | bytes 4718596
  159.9 120.5 %all-gather.10.cloned.1.call-start = ((), (), s32[]{:S(2)}) async-start(), calls=%async_computation.6 | async-start | bytes 7077888 | tf_op jit(solution)/shard_map/all_gather | solution.py:38
  160.5 164.1 %reduce-scatter.6.cloned.1.call-start = ((), (), s32[]{:S(2)}) async-start(), calls=%async_computation.7 | async-start | bytes 1966080 | tf_op jit(solution)/shard_map/reduce_scatter | solution.py:44
  297.9 63.2 %all-gather.12.cloned.1.call-start = ((), (), s32[]{:S(2)}) async-start(), calls=%async_computation.8 | async-start | bytes 1966080 | tf_op jit(solution)/shard_map/all_gather | solution.py:72
  325.6 5.3 %collective-permute-start.2 = (bf16[256,8]{1,0:T(8,128)(2,1)S(1)}, bf16[256,8]{1,0:T(8,128)(2,1)S(1)}, u32[]{:S(2)}, u32[]{:S(2)}) collective-permute-start(bf16[256,8]{1,0:T(8,128)(2,1)S(1)} %get-tuple-element.22), channel_id=1, source_target_pairs={{0,4},{4,8},{8,12},{12,16},{16,20},{20,24},{24,28},{1,5},{5,9},{9,... | collective-permute-start | bytes 12296 | tf_op jit(solution)/shard_map/ppermute | solution.py:17
  328.9 6.2 %collective-permute-start.3 = (bf16[256,8]{1,0:T(8,128)(2,1)S(1)}, bf16[256,8]{1,0:T(8,128)(2,1)S(1)}, u32[]{:S(2)}, u32[]{:S(2)}) collective-permute-start(bf16[256,8]{1,0:T(8,128)(2,1)S(1)} %get-tuple-element.23), channel_id=1, source_target_pairs={{4,0},{8,4},{12,8},{16,12},{20,16},{24,20},{28,24},{5,1},{9,5},{13... | collective-permute-start | bytes 12296 | tf_op jit(solution)/shard_map/ppermute | solution.py:18
  341.3 69.2 %reduce-scatter.8.cloned.1.call-start = ((), (), s32[]{:S(2)}) async-start(), calls=%async_computation.9 | async-start | bytes 1966080 | tf_op jit(solution)/shard_map/reduce_scatter | solution.py:44
  361.1 2.4 copy-start.4
  381.2 65.8 %all-gather.14.cloned.1.call-start = ((), (), s32[]{:S(2)}) async-start(), calls=%async_computation.10 | async-start | bytes 1966080 | tf_op jit(solution)/shard_map/all_gather | solution.py:72
  411.5 5.3 %collective-permute-start.4 = (bf16[256,8]{1,0:T(8,128)(2,1)S(1)}, bf16[256,8]{1,0:T(8,128)(2,1)S(1)}, u32[]{:S(2)}, u32[]{:S(2)}) collective-permute-start(bf16[256,8]{1,0:T(8,128)(2,1)S(1)} %get-tuple-element.20), channel_id=1, source_target_pairs={{0,4},{4,8},{8,12},{12,16},{16,20},{20,24},{24,28},{1,5},{5,9},{9,... | collective-permute-start | bytes 12296 | tf_op jit(solution)/shard_map/ppermute | solution.py:17
  414.8 6.2 %collective-permute-start.5 = (bf16[256,8]{1,0:T(8,128)(2,1)S(1)}, bf16[256,8]{1,0:T(8,128)(2,1)S(1)}, u32[]{:S(2)}, u32[]{:S(2)}) collective-permute-start(bf16[256,8]{1,0:T(8,128)(2,1)S(1)} %get-tuple-element.21), channel_id=1, source_target_pairs={{4,0},{8,4},{12,8},{16,12},{20,16},{24,20},{28,24},{5,1},{9,5},{13... | collective-permute-start | bytes 12296 | tf_op jit(solution)/shard_map/ppermute | solution.py:18
  447.0 2.4 copy-start.5
Sparse Core Ops, SparseCore 0:
  9.4 102.1 all-gather.5
  116.8 26.2 reduce-scatter.3
  160.1 19.5 all-gather.7
  181.7 98.6 all-gather.9
  298.0 26.4 reduce-scatter.5
  341.4 19.6 all-gather.11
  381.3 29.1 reduce-scatter.7
  427.3 19.6 all-gather.13
where the time goes:
time: 469 us; the launch traced here: 468 us
  waiting for transfers between devices  359 us (77%)
  matrix products  39.2 us (8%)
  other arithmetic  20.4 us (4%)
  blocking collectives  17.7 us (4%)
  starting transfers between devices  14.5 us (3%)
  between operations  13.8 us (3%)
    all_gather x1, waiting for transfers between devices, on_device(): lax.all_gather(in_proj, 'sp', axis=2, tiled=True)  104 us
    all_gather x1, waiting for transfers between devices, on_device(): lax.all_gather(out_proj, 'sp', axis=1, tiled=True)  98.7 us
    reduce_scatter x3, waiting for transfers between devices, on_device(): lax.psum_scatter(lax.dot_general(in_block, stream, (((0,), (1,)), ((), ()...  82.1 us
    all_gather x3, waiting for transfers between devices, on_device(): all_differ = lax.all_gather(differ, 'tp', axis=0, tiled=True)  58.3 us
    psum x3, blocking collectives, on_device(): lax.psum((jnp.sum(resid, axis=1), jnp.sum(resid * resid, axis=1)), 'tp')  17.7 us
    dot_general x3, matrix products, on_device(): lax.dot_general(in_block, stream, (((0,), (1,)), ((), ())), preferred_ele...  16.8 us
    dot_general x3, matrix products, on_device(): lax.dot_general(mixed_all, out_block, (((0,), (0,)), ((), ())), preferred...  16 us
    convert_element_type x3, other arithmetic, on_device(): differ = (pooled - projected.astype(jnp.float32)).astype(jnp.bfloat16)  15 us
  transfers between devices with their start and end apart: 14, of which 14 were waited for; matrix products, arithmetic and copies ran while one was open for 0% of the time, Pallas kernels for 0%

commit v1 on v0

--- a/solution.py
+++ b/solution.py
@@ -5,6 +5,11 @@
 
 pool_windows = (2, 4, 8, 16)
 norm_eps = 1e-05
+
+
+def advance_the_blocks(inp, device_axis, d_out):
+    near = lax.all_gather(inp, axis_name=device_axis)
+    return jnp.concatenate(near, axis=d_out)
 
 
 def padded(array, sides, width):
@@ -35,7 +40,7 @@
     chan_groups = (lax.axis_index("tp") * chan_share + jnp.arange(chan_share)) // group_width
     in_all, out_all = (
         lax.all_gather(in_proj, "sp", axis=2, tiled=True),
-        lax.all_gather(out_proj, "sp", axis=1, tiled=True),
+        advance_the_blocks(out_proj, "sp", 1),
     )
     stream = tokens
     for layer_idx in range(layer_count):

time: 469 us -> 455 us (0.970)
  waiting for transfers between devices: 359 us -> 341 us
  local copies, waits for them, and re-layouts: 3.32 us -> 9.37 us
    all_gather x1, waiting for transfers between devices: 98.7 us -> 84 us  [advance_the_blocks(): near = lax.all_gather(inp, axis_name=device_axis)]
    slice x0 -> x1, local copies, waits for them, and re-layouts: none -> 5.91 us  [on_device(): out_block = out_all[layer_idx]]
    all_gather x3, waiting for transfers between devices: 58.3 us -> 52.8 us  [on_device(): all_differ = lax.all_gather(differ, 'tp', axis=0, tiled=True)]
  transfers between devices with their start and end apart: 14 -> 14, of which waited for: 14 -> 14; matrix products, arithmetic and copies ran while one was open for 0% -> 3% of each run, Pallas kernels for 0% -> 0%
where the time goes in v1:
time: 455 us; the launch traced here: 454 us
  waiting for transfers between devices  341 us (75%)
  matrix products  37.2 us (8%)
  other arithmetic  20.3 us (4%)
  blocking collectives  17.9 us (4%)
  starting transfers between devices  14.7 us (3%)
  between operations  13.8 us (3%)
  local copies, waits for them, and re-layouts  9.37 us (2%)
    all_gather x1, waiting for transfers between devices, on_device(): lax.all_gather(in_proj, 'sp', axis=2, tiled=True)  104 us
    reduce_scatter x3, waiting for transfers between devices, on_device(): lax.psum_scatter(lax.dot_general(in_block, stream, (((0,), (1,)), ((), ()...  84 us
    all_gather x1, waiting for transfers between devices, advance_the_blocks(): near = lax.all_gather(inp, axis_name=device_axis)  84 us
    all_gather x3, waiting for transfers between devices, on_device(): all_differ = lax.all_gather(differ, 'tp', axis=0, tiled=True)  52.8 us
    psum x3, blocking collectives, on_device(): lax.psum((jnp.sum(resid, axis=1), jnp.sum(resid * resid, axis=1)), 'tp')  17.9 us
    dot_general x3, matrix products, on_device(): lax.dot_general(in_block, stream, (((0,), (1,)), ((), ())), preferred_ele...  16.8 us
    convert_element_type x3, other arithmetic, on_device(): differ = (pooled - projected.astype(jnp.float32)).astype(jnp.bfloat16)  14.9 us
    dot_general x3, matrix products, on_device(): lax.dot_general(mixed_all, out_block, (((0,), (0,)), ((), ())), preferred...  13.5 us
  transfers between devices with their start and end apart: 14, of which 14 were waited for; matrix products, arithmetic and copies ran while one was open for 3% of the time, Pallas kernels for 0%

profile of v1, /device:TPU:0, one launch (start us, length us, event | category | flops | bytes accessed | tf_op | source)
XLA Modules:
  0.0 454.0 jit_solution(15600836041073174516)
XLA Ops:
  6.5 0.7 all-gather.7.cloned.1.call-update
  7.3 0.0 reduce-scatter.4.cloned.1.call-start
  7.3 104.3 %all-gather.7.cloned.1.call-done = bf16[3,1024,1024]{2,1,0:T(8,128)(2,1)} async-done(((bf16[3,1024,128]{2,1,0:T(8,128)(2,1)}), bf16[3,1024,1024]{2,1,0:T(8,128)(2,1)}) %all-gather.7.cloned.1.call-update) | async-done | bytes 6291472 | tf_op jit(solution)/shard_map/all_gather | solution.py:42
  111.6 5.0 %fusion.3 = bf16[1024,768]{1,0:T(8,128)(2,1)} fusion(bf16[768,1024]{1,0:T(8,128)(2,1)} %param.7, bf16[3,1024,1024]{2,1,0:T(8,128)(2,1)} %all-gather.7.cloned.1.call-done), kind=kOutput, calls=%fused_computation.18 | convolution fusion | flops 1611399168 | bytes 5242880 | tf_op jit(solution)/shard_map/dot_general | solution.py:50
  116.6 0.0 reduce-scatter.4.cloned.1.call-update
  116.7 0.0 all-gather.15.cloned.1.call-start
  116.7 0.7 all-gather.15.cloned.1.call-update
  117.4 0.0 all-gather.9.cloned.1.call-start
  117.5 25.5 %reduce-scatter.4.cloned.1.call-done = bf16[256,768]{1,0:T(8,128)(2,1)} async-done(((bf16[1024,768]{1,0:T(8,128)(2,1)}), bf16[256,768]{1,0:T(8,128)(2,1)}) %reduce-scatter.4.cloned.1.call-update) | async-done | bytes 393232 | tf_op jit(solution)/shard_map/reduce_scatter | solution.py:49
  143.0 1.0 fusion.56
  144.0 3.4 collective-permute-start
  147.4 1.3 collective-permute-start.1
  148.7 0.6 collective-permute-done
  149.3 4.3 collective-permute-done.1
  153.6 1.2 maximum_convert_fusion
  154.8 0.0 copy-start.1
  154.8 0.0 copy-start.2
  154.8 0.0 copy-start.3
  154.8 5.0 %fusion.41 = bf16[256,768]{1,0:T(8,128)(2,1)} fusion(bf16[256,768]{1,0:T(8,128)(2,1)} %reduce-scatter.4.cloned.1.call-done, f32[256,784]{1,0:T(8,128)S(1)} %maximum_convert_fusion, f32[768]{0:T(1024)S(1)} %get-tuple-element.44, f32[768]{0:T(1024)S(1)} %get-tuple-element.45, f32[768]{0:T(1024)S(1)} %get-tuple-element.46, f32[768]{0:T(1024)S(1)} %get-tuple-element.47, ...), kind=kLoop, calls=%fused_computation.77 | loop fusion | flops 7274496 | bytes 13382656 | tf_op jit(solution)/shard_map/convert_element_type | solution.py:76
  159.8 0.0 all-gather.9.cloned.1.call-update
  159.8 0.0 reduce-scatter.6.cloned.1.call-start
  159.9 0.0 copy-done.1
  160.0 84.0 %all-gather.15.cloned.1.call-done = bf16[24,128,1024]{2,1,0:T(8,128)(2,1)} async-done(((bf16[3,128,1024]{2,1,0:T(8,128)(2,1)}), bf16[24,128,1024]{2,1,0:T(8,128)(2,1)}) %all-gather.15.cloned.1.call-update) | async-done | bytes 6291472 | tf_op jit(solution)/shard_map/all_gather | solution.py:11
  244.0 5.9 %fusion.53 = (bf16[1,8,128,1024]{3,2,0,1:T(8,128)(2,1)}, bf16[1,8,128,1024]{3,2,0,1:T(8,128)(2,1)S(1)}, bf16[1,8,128,1024]{3,2,0,1:T(8,128)(2,1)}) fusion(bf16[3,8,128,1024]{3,2,0,1:T(8,128)(2,1)} %bitcast.69), kind=kLoop, calls=%fused_computation.114 | loop fusion | bytes 12582912 | tf_op jit(solution)/shard_map/slice | solution.py:48
  249.9 13.3 %all-gather.9.cloned.1.call-done = bf16[1024,768]{1,0:T(8,128)(2,1)} async-done(((bf16[256,768]{1,0:T(8,128)(2,1)}), bf16[1024,768]{1,0:T(8,128)(2,1)}) %all-gather.9.cloned.1.call-update) | async-done | bytes 1572880 | tf_op jit(solution)/shard_map/all_gather | solution.py:77
  263.2 2.3 multiply_convert_fusion.2
  265.6 0.3 copy-done.4
  265.9 3.9 fusion.52
  269.8 6.0 %all-reduce.2 = (f32[768]{0:T(1024)S(1)}, f32[768]{0:T(1024)S(1)}) all-reduce(f32[768]{0:T(1024)S(1)} %get-tuple-element.10, f32[768]{0:T(1024)S(1)} %get-tuple-element.9), channel_id=1, replica_groups=mesh['sp'=8,'tp'=4] {'tp'}, use_global_device_ids=true, to_apply=%region_4.5 | all-reduce | flops 1536 | bytes 12288 | tf_op jit(solution)/shard_map/psum | solution.py:87
  275.8 5.9 %fusion.7 = bf16[1024,768]{1,0:T(8,128)(2,1)} fusion(bf16[3,1024,1024]{2,1,0:T(8,128)(2,1)} %all-gather.7.cloned.1.call-done, f32[768,1024]{1,0:T(8,128)} %get-tuple-element.41, f32[1024]{0:T(1024)S(1)} %bitcast.87, f32[1024]{0:T(1024)S(1)} %bitcast.85, f32[768]{0:T(1024)S(1)} %get-tuple-element.40, f32[768]{0:T(1024)S(1)} %get-tuple-element.39), kind=kOutput, calls=%fused_computation.22 | convolution fusion | flops 1615331328 | bytes 6830080 | tf_op jit(solution)/shard_map/dot_general | solution.py:50
  281.7 0.0 reduce-scatter.6.cloned.1.call-update
  281.7 0.0 all-gather.11.cloned.1.call-start
  281.8 29.2 %reduce-scatter.6.cloned.1.call-done = bf16[256,768]{1,0:T(8,128)(2,1)} async-done(((bf16[1024,768]{1,0:T(8,128)(2,1)}), bf16[256,768]{1,0:T(8,128)(2,1)}) %reduce-scatter.6.cloned.1.call-update) | async-done | bytes 393232 | tf_op jit(solution)/shard_map/reduce_scatter | solution.py:49
  311.0 1.0 fusion.55
  311.9 3.4 collective-permute-start.2
  315.3 1.5 collective-permute-start.3
  316.8 0.4 collective-permute-done.2
  317.2 4.3 collective-permute-done.3
  321.5 1.2 maximum_convert_fusion.1
  322.7 5.0 %fusion.42 = bf16[256,768]{1,0:T(8,128)(2,1)} fusion(bf16[256,768]{1,0:T(8,128)(2,1)} %reduce-scatter.6.cloned.1.call-done, f32[256,784]{1,0:T(8,128)S(1)} %maximum_convert_fusion.1, f32[768]{0:T(1024)S(1)} %get-tuple-element.44, f32[768]{0:T(1024)S(1)} %get-tuple-element.45, f32[768]{0:T(1024)S(1)} %get-tuple-element.46, f32[768]{0:T(1024)S(1)} %get-tuple-element.47, ...), kind=kLoop, calls=%fused_computation.78 | loop fusion | flops 7274496 | bytes 13382656 | tf_op jit(solution)/shard_map/convert_element_type | solution.py:76
  327.7 0.0 all-gather.11.cloned.1.call-update
  327.7 0.0 reduce-scatter.8.cloned.1.call-start
  327.8 19.7 %all-gather.11.cloned.1.call-done = bf16[1024,768]{1,0:T(8,128)(2,1)} async-done(((bf16[256,768]{1,0:T(8,128)(2,1)}), bf16[1024,768]{1,0:T(8,128)(2,1)}) %all-gather.11.cloned.1.call-update) | async-done | bytes 1572880 | tf_op jit(solution)/shard_map/all_gather | solution.py:77
  347.5 2.3 multiply_convert_fusion.1
  349.8 0.2 copy-done.5
  350.0 4.4 fusion.51
  354.4 6.0 %all-reduce.1 = (f32[768]{0:T(1024)S(1)}, f32[768]{0:T(1024)S(1)}) all-reduce(f32[768]{0:T(1024)S(1)} %get-tuple-element.8, f32[768]{0:T(1024)S(1)} %get-tuple-element.7), channel_id=1, replica_groups=mesh['sp'=8,'tp'=4] {'tp'}, use_global_device_ids=true, to_apply=%region_9.10 | all-reduce | flops 1536 | bytes 12288 | tf_op jit(solution)/shard_map/psum | solution.py:87
  360.3 5.9 %fusion.6 = bf16[1024,768]{1,0:T(8,128)(2,1)} fusion(bf16[3,1024,1024]{2,1,0:T(8,128)(2,1)} %all-gather.7.cloned.1.call-done, f32[768,1024]{1,0:T(8,128)} %get-tuple-element.42, f32[1024]{0:T(1024)S(1)} %bitcast.83, f32[1024]{0:T(1024)S(1)} %bitcast.81, f32[768]{0:T(1024)S(1)} %get-tuple-element.38, f32[768]{0:T(1024)S(1)} %get-tuple-element.37), kind=kOutput, calls=%fused_computation.21 | convolution fusion | flops 1615331328 | bytes 6830080 | tf_op jit(solution)/shard_map/dot_general | solution.py:50
  366.2 0.0 reduce-scatter.8.cloned.1.call-update
  366.3 0.0 all-gather.13.cloned.1.call-start
  366.3 29.2 %reduce-scatter.8.cloned.1.call-done = bf16[256,768]{1,0:T(8,128)(2,1)} async-done(((bf16[1024,768]{1,0:T(8,128)(2,1)}), bf16[256,768]{1,0:T(8,128)(2,1)}) %reduce-scatter.8.cloned.1.call-update) | async-done | bytes 393232 | tf_op jit(solution)/shard_map/reduce_scatter | solution.py:49
  395.5 1.0 fusion.54
  396.5 3.4 collective-permute-start.4
  399.9 1.5 collective-permute-start.5
  401.4 0.4 collective-permute-done.4
  401.8 4.3 collective-permute-done.5
  406.0 1.2 maximum_convert_fusion.2
  407.3 5.0 %fusion.43 = bf16[256,768]{1,0:T(8,128)(2,1)} fusion(bf16[256,768]{1,0:T(8,128)(2,1)} %reduce-scatter.8.cloned.1.call-done, f32[256,784]{1,0:T(8,128)S(1)} %maximum_convert_fusion.2, f32[768]{0:T(1024)S(1)} %get-tuple-element.44, f32[768]{0:T(1024)S(1)} %get-tuple-element.45, f32[768]{0:T(1024)S(1)} %get-tuple-element.46, f32[768]{0:T(1024)S(1)} %get-tuple-element.47, ...), kind=kLoop, calls=%fused_computation.79 | loop fusion | flops 7274496 | bytes 13382656 | tf_op jit(solution)/shard_map/convert_element_type | solution.py:76
  412.2 0.0 all-gather.13.cloned.1.call-update
  412.2 19.8 %all-gather.13.cloned.1.call-done = bf16[1024,768]{1,0:T(8,128)(2,1)} async-done(((bf16[256,768]{1,0:T(8,128)(2,1)}), bf16[1024,768]{1,0:T(8,128)(2,1)}) %all-gather.13.cloned.1.call-update) | async-done | bytes 1572880 | tf_op jit(solution)/shard_map/all_gather | solution.py:77
  432.0 2.2 multiply_convert_fusion
  434.2 5.2 %fusion.50 = (f32[768]{0:T(1024)S(1)}, f32[768]{0:T(1024)S(1)}, f32[768,1024]{1,0:T(8,128)S(1)}) fusion(bf16[1024,768]{1,0:T(8,128)(2,1)S(1)} %bitcast.75, bf16[1024,1024]{1,0:T(8,128)(2,1)} %bitcast.70, f32[1024]{0:T(1024)S(1)} %bitcast.84, f32[1024]{0:T(1024)S(1)} %bitcast.82, f32[768]{0:T(1024)S(1)} %get-tuple-element.38, ...), kind=kOutput, calls=%fused_computation.111 | convolution fusion | flops 1619261952 | bytes 9981952 | tf_op jit(solution)/shard_map/dot_general | solution.py:83
  439.4 6.0 %all-reduce = (f32[768]{0:T(1024)S(1)}, f32[768]{0:T(1024)S(1)}) all-reduce(f32[768]{0:T(1024)S(1)} %get-tuple-element.6, f32[768]{0:T(1024)S(1)} %get-tuple-element.5), channel_id=1, replica_groups=mesh['sp'=8,'tp'=4] {'tp'}, use_global_device_ids=true, to_apply=%region_14.15 | all-reduce | flops 1536 | bytes 12288 | tf_op jit(solution)/shard_map/psum | solution.py:87
  445.4 1.7 add_convert_fusion
  (20 shorter events, 0.2 us)
Async XLA Ops:
  6.5 105.1 %all-gather.7.cloned.1.call-start = ((), (), s32[]{:S(2)}) async-start(), calls=%async_computation.3 | async-start | bytes 7077888 | tf_op jit(solution)/shard_map/all_gather | solution.py:42
  7.3 135.8 %reduce-scatter.4.cloned.1.call-start = ((), (), s32[]{:S(2)}) async-start(), calls=%async_computation.4 | async-start | bytes 1966080 | tf_op jit(solution)/shard_map/reduce_scatter | solution.py:49
  116.7 127.3 %all-gather.15.cloned.1.call-start = ((), (), s32[]{:S(2)}) async-start(), calls=%async_computation.10 | async-start | bytes 7077888 | tf_op jit(solution)/shard_map/all_gather | solution.py:11
  117.4 145.8 %all-gather.9.cloned.1.call-start = ((), (), s32[]{:S(2)}) async-start(), calls=%async_computation.5 | async-start | bytes 1966080 | tf_op jit(solution)/shard_map/all_gather | solution.py:77
  144.0 5.3 %collective-permute-start = (bf16[256,8]{1,0:T(8,128)(2,1)S(1)}, bf16[256,8]{1,0:T(8,128)(2,1)S(1)}, u32[]{:S(2)}, u32[]{:S(2)}) collective-permute-start(bf16[256,8]{1,0:T(8,128)(2,1)S(1)} %get-tuple-element.27), channel_id=1, source_target_pairs={{0,4},{4,8},{8,12},{12,16},{16,20},{20,24},{24,28},{1,5},{5,9},{9,... | collective-permute-start | bytes 12296 | tf_op jit(solution)/shard_map/ppermute | solution.py:22
  147.4 6.2 %collective-permute-start.1 = (bf16[256,8]{1,0:T(8,128)(2,1)S(1)}, bf16[256,8]{1,0:T(8,128)(2,1)S(1)}, u32[]{:S(2)}, u32[]{:S(2)}) collective-permute-start(bf16[256,8]{1,0:T(8,128)(2,1)S(1)} %get-tuple-element.28), channel_id=1, source_target_pairs={{4,0},{8,4},{12,8},{16,12},{20,16},{24,20},{28,24},{5,1},{9,5},{13... | collective-permute-start | bytes 12296 | tf_op jit(solution)/shard_map/ppermute | solution.py:23
  154.8 5.1 %copy-start.1 = (f32[3,1024]{1,0:T(4,128)S(1)}, f32[3,1024]{1,0:T(4,128)}, u32[]{:S(2)}) copy-start(f32[3,1024]{1,0:T(4,128)} %param.10) | copy-start | bytes 36868
  154.8 5.1 %copy-start.2 = (f32[3,1024]{1,0:T(4,128)S(1)}, f32[3,1024]{1,0:T(4,128)}, u32[]{:S(2)}) copy-start(f32[3,1024]{1,0:T(4,128)} %param.12) | copy-start | bytes 36868
  154.8 5.1 %copy-start.3 = (f32[3,1024]{1,0:T(4,128)S(1)}, f32[3,1024]{1,0:T(4,128)}, u32[]{:S(2)}) copy-start(f32[3,1024]{1,0:T(4,128)} %param.13) | copy-start | bytes 36868
  159.8 151.2 %reduce-scatter.6.cloned.1.call-start = ((), (), s32[]{:S(2)}) async-start(), calls=%async_computation.6 | async-start | bytes 1966080 | tf_op jit(solution)/shard_map/reduce_scatter | solution.py:49
  263.2 2.4 copy-start
  263.2 2.7 copy-start.4
  281.7 65.7 %all-gather.11.cloned.1.call-start = ((), (), s32[]{:S(2)}) async-start(), calls=%async_computation.7 | async-start | bytes 1966080 | tf_op jit(solution)/shard_map/all_gather | solution.py:77
  311.9 5.3 %collective-permute-start.2 = (bf16[256,8]{1,0:T(8,128)(2,1)S(1)}, bf16[256,8]{1,0:T(8,128)(2,1)S(1)}, u32[]{:S(2)}, u32[]{:S(2)}) collective-permute-start(bf16[256,8]{1,0:T(8,128)(2,1)S(1)} %get-tuple-element.25), channel_id=1, source_target_pairs={{0,4},{4,8},{8,12},{12,16},{16,20},{20,24},{24,28},{1,5},{5,9},{9,... | collective-permute-start | bytes 12296 | tf_op jit(solution)/shard_map/ppermute | solution.py:22
  315.3 6.2 %collective-permute-start.3 = (bf16[256,8]{1,0:T(8,128)(2,1)S(1)}, bf16[256,8]{1,0:T(8,128)(2,1)S(1)}, u32[]{:S(2)}, u32[]{:S(2)}) collective-permute-start(bf16[256,8]{1,0:T(8,128)(2,1)S(1)} %get-tuple-element.26), channel_id=1, source_target_pairs={{4,0},{8,4},{12,8},{16,12},{20,16},{24,20},{28,24},{5,1},{9,5},{13... | collective-permute-start | bytes 12296 | tf_op jit(solution)/shard_map/ppermute | solution.py:23
  327.7 67.8 %reduce-scatter.8.cloned.1.call-start = ((), (), s32[]{:S(2)}) async-start(), calls=%async_computation.8 | async-start | bytes 1966080 | tf_op jit(solution)/shard_map/reduce_scatter | solution.py:49
  347.5 2.5 copy-start.5
  366.3 65.7 %all-gather.13.cloned.1.call-start = ((), (), s32[]{:S(2)}) async-start(), calls=%async_computation.9 | async-start | bytes 1966080 | tf_op jit(solution)/shard_map/all_gather | solution.py:77
  396.5 5.3 %collective-permute-start.4 = (bf16[256,8]{1,0:T(8,128)(2,1)S(1)}, bf16[256,8]{1,0:T(8,128)(2,1)S(1)}, u32[]{:S(2)}, u32[]{:S(2)}) collective-permute-start(bf16[256,8]{1,0:T(8,128)(2,1)S(1)} %get-tuple-element.23), channel_id=1, source_target_pairs={{0,4},{4,8},{8,12},{12,16},{16,20},{20,24},{24,28},{1,5},{5,9},{9,... | collective-permute-start | bytes 12296 | tf_op jit(solution)/shard_map/ppermute | solution.py:22
  399.9 6.2 %collective-permute-start.5 = (bf16[256,8]{1,0:T(8,128)(2,1)S(1)}, bf16[256,8]{1,0:T(8,128)(2,1)S(1)}, u32[]{:S(2)}, u32[]{:S(2)}) collective-permute-start(bf16[256,8]{1,0:T(8,128)(2,1)S(1)} %get-tuple-element.24), channel_id=1, source_target_pairs={{4,0},{8,4},{12,8},{16,12},{20,16},{24,20},{28,24},{5,1},{9,5},{13... | collective-permute-start | bytes 12296 | tf_op jit(solution)/shard_map/ppermute | solution.py:23
Sparse Core Ops, SparseCore 0:
  9.4 102.1 all-gather.6
  116.8 26.2 reduce-scatter.3
  145.2 98.6 all-gather.14
  245.4 17.7 all-gather.8
  281.8 29.1 reduce-scatter.5
  327.8 19.5 all-gather.10
  366.4 29.1 reduce-scatter.7
  412.4 19.6 all-gather.12
